TPU v7x, 32 devices: a whole 2x2x4 slice. The times are simulated.
32 devices in a mesh: ep: 8 (over z, core), tp: 4 (over y, x).
Axes of the slice: x: 2, y: 2, z: 4, core: 2. Of those that a mesh axis runs over, the one named last changes fastest.
Arguments:
- outer_gate: bfloat16 [1024, 2048], P('ep', 'tp'), may hold values from -6 to 6
- inner_gate: bfloat16 [1024, 2048], P('ep', 'tp'), may hold values from -6 to 6
- conv_value: bfloat16 [1024, 2048], P('ep', 'tp'), may hold values from -6 to 6
- conv_taps: bfloat16 [3, 2048], P(None, 'tp'), may hold values from -3.5 to 3.5
- mix_out: bfloat16 [2048, 2048], P(None, 'tp')
- gain_mixer: bfloat16 [2048], P('tp'), may hold values from 0.099609375 to 1.8984375
- bias_mixer: bfloat16 [2048], P('tp'), may hold values from -3 to 3
- moe_input: bfloat16 [1024, 2048], P('ep'), may hold values from -6 to 6
- route_ids: int32 [1024, 4], P('ep'), may hold values from 0 to 7, all different within a row; in each aligned block of 128 rows (0 to 127, 128 to 255, ...) at most 96 rows name the same one
- route_weights: float32 [1024, 4], P('ep'), may hold values from 0.1 to 1.2
- expert_gate: bfloat16 [8, 2048, 2048], P('ep', None, 'tp'), may hold values from -0.125 to 0.125
- expert_up: bfloat16 [8, 2048, 2048], P('ep', None, 'tp'), may hold values from -0.125 to 0.125
- expert_down: bfloat16 [8, 2048, 2048], P('ep', None, 'tp')
- shared_gate: bfloat16 [2048, 2048], P(None, 'tp'), may hold values from -0.125 to 0.125
- shared_up: bfloat16 [2048, 2048], P(None, 'tp'), may hold values from -0.125 to 0.125
- shared_down: bfloat16 [2048, 2048], P(None, 'tp')
- gain_experts: bfloat16 [2048], P('tp'), may hold values from 0.099609375 to 1.8984375
- bias_experts: bfloat16 [2048], P('tp'), may hold values from -3 to 3
Outputs:
- out_mixer: bfloat16 [1024, 2048], P('ep', 'tp')
- out_experts: bfloat16 [1024, 2048], P('ep', 'tp')
Inputs may be any that keep to these rules, and one draw needn't show every extreme that they name: `route_ids`: each row names 4 different experts. Among the rows of one index of ep (aligned blocks of 128 rows) no expert is named more than 96 times, a bound that some block reaches.
All inputs are finite; a program needn't handle non-finite values.
Results may differ from a plain program's by a relative error of at most 0.0055.
Values may be sent and summed in bfloat16 or wider, within the bound.
A program may use at most 64 MiB of HBM per device.

v0:
```python
import jax
import jax.numpy as jnp
from jax import lax
from jax.sharding import PartitionSpec as P

SEQS = 1


def shifted(block, axis, distance):
    devices = range(lax.axis_size(axis))
    route = [(i - distance, i) for i in devices if i - distance in devices]
    return lax.ppermute(block, axis, route)


def finish(values, totals, squares, full_width, gain, offset_bias):
    average = (totals / full_width)[:, None]
    spread = (squares / full_width)[:, None] - average * average
    scaled = (values - average) * lax.rsqrt(spread + 1e-05)
    return (scaled * gain.astype(jnp.float32) + offset_bias.astype(jnp.float32)).astype(
        jnp.bfloat16
    )


def on_device(
    outer_gate,
    inner_gate,
    conv_value,
    conv_taps,
    mix_out,
    gain_mixer,
    bias_mixer,
    moe_input,
    route_ids,
    route_weights,
    expert_gate,
    expert_up,
    expert_down,
    shared_gate,
    shared_up,
    shared_down,
    gain_experts,
    bias_experts,
):
    token_rows = outer_gate.shape[0]
    column_count = outer_gate.shape[1]
    ep_count = lax.axis_size("ep")
    tp_count = lax.axis_size("tp")
    taps_count = conv_taps.shape[0]
    product = (inner_gate.astype(jnp.float32) * conv_value.astype(jnp.float32)).astype(jnp.bfloat16)
    border = shifted(product[token_rows - (taps_count - 1) :], "ep", 1)
    extended = jnp.concatenate([border, product], axis=0).astype(jnp.float32)
    seq_length = token_rows * ep_count // SEQS
    places = (
        lax.axis_index("ep") * token_rows + jnp.arange(token_rows, dtype=jnp.int32)
    ) % seq_length
    convolved = jnp.zeros((token_rows, column_count), jnp.float32)
    for offset in range(taps_count):
        delay_rows = taps_count - 1 - offset
        delayed = extended[offset : offset + token_rows]
        kept_mask = (places >= delay_rows).astype(jnp.float32)[:, None]
        convolved = convolved + conv_taps[offset].astype(jnp.float32)[None, :] * delayed * kept_mask
    weighted_in = (outer_gate.astype(jnp.float32) * convolved).astype(jnp.bfloat16)
    block = mix_out
    mixed = jnp.dot(
        lax.all_gather(weighted_in, "tp", axis=1, tiled=True),
        block,
        preferred_element_type=jnp.float32,
    )
    topk_count = route_ids.shape[1]
    local_experts = expert_gate.shape[0]
    expert_count = local_experts * ep_count
    capacity = max(2, 3 * token_rows * topk_count // (2 * expert_count))
    flat_ids = route_ids.reshape(-1)
    marks = (flat_ids[:, None] == jnp.arange(expert_count, dtype=jnp.int32)[None, :]).astype(
        jnp.int32
    )
    ranks = jnp.sum((jnp.cumsum(marks, axis=0) - marks) * marks, axis=1)
    targets = flat_ids * capacity + ranks
    sources = jnp.arange(flat_ids.shape[0], dtype=jnp.int32) // topk_count
    sent_rows = lax.dynamic_slice_in_dim(
        moe_input, lax.axis_index("tp") * column_count, column_count, 1
    )
    buffer_rows = jnp.zeros((expert_count * capacity, sent_rows.shape[1]), jnp.bfloat16)
    buffer_rows = buffer_rows.at[targets].set(sent_rows[sources])
    sectioned = buffer_rows.reshape(ep_count, local_experts * capacity, sent_rows.shape[1])
    arrived = lax.all_to_all(sectioned, "ep", split_axis=0, concat_axis=0, tiled=True)
    arrived = lax.all_gather(arrived, "tp", axis=2, tiled=True)
    expert_rows = arrived.reshape(ep_count, local_experts, capacity, arrived.shape[2])
    gate_value = jnp.einsum(
        "secd,edf->secf", expert_rows, expert_gate, preferred_element_type=jnp.float32
    )
    up_value = jnp.einsum(
        "secd,edf->secf", expert_rows, expert_up, preferred_element_type=jnp.float32
    )
    hidden = (jax.nn.silu(gate_value) * up_value).astype(jnp.bfloat16)
    flat_hidden = hidden.reshape(expert_count * capacity, hidden.shape[3])
    shared_gate_value = jnp.dot(moe_input, shared_gate, preferred_element_type=jnp.float32)
    shared_up_value = jnp.dot(moe_input, shared_up, preferred_element_type=jnp.float32)
    shared_hidden = (jax.nn.silu(shared_gate_value) * shared_up_value).astype(jnp.bfloat16)
    piece = lax.all_gather(flat_hidden, "tp", axis=1, tiled=True)
    block = expert_down
    shaped = piece.reshape(ep_count, local_experts, capacity, piece.shape[1])
    routed_sum = jnp.einsum("secf,efd->secd", shaped, block, preferred_element_type=jnp.float32)
    block = shared_down
    shared_sum = jnp.dot(
        lax.all_gather(shared_hidden, "tp", axis=1, tiled=True),
        block,
        preferred_element_type=jnp.float32,
    )
    expert_out = routed_sum.astype(jnp.bfloat16).reshape(
        ep_count, local_experts * capacity, column_count
    )
    returned = lax.all_to_all(expert_out, "ep", split_axis=0, concat_axis=0, tiled=True)
    picked = returned.reshape(expert_count * capacity, column_count)[targets].astype(jnp.float32)
    weighted = picked.reshape(token_rows, topk_count, column_count) * route_weights[:, :, None]
    combined = jnp.sum(weighted, axis=1) + shared_sum
    mixer_total, mixer_square, expert_total, expert_square = lax.psum(
        (
            jnp.sum(mixed, axis=1),
            jnp.sum(mixed * mixed, axis=1),
            jnp.sum(combined, axis=1),
            jnp.sum(combined * combined, axis=1),
        ),
        "tp",
    )
    full_width = column_count * tp_count
    out_mixer = finish(mixed, mixer_total, mixer_square, full_width, gain_mixer, bias_mixer)
    out_experts = finish(
        combined, expert_total, expert_square, full_width, gain_experts, bias_experts
    )
    return (out_mixer, out_experts)


def solution(mesh):
    in_specs = (
        P("ep", "tp"),
        P("ep", "tp"),
        P("ep", "tp"),
        P(None, "tp"),
        P(None, "tp"),
        P("tp"),
        P("tp"),
        P("ep", None),
        P("ep", None),
        P("ep", None),
        P("ep", None, "tp"),
        P("ep", None, "tp"),
        P("ep", None, "tp"),
        P(None, "tp"),
        P(None, "tp"),
        P(None, "tp"),
        P("tp"),
        P("tp"),
    )
    out_specs = (P("ep", "tp"), P("ep", "tp"))
    return jax.shard_map(
        on_device, mesh=mesh, in_specs=in_specs, out_specs=out_specs, check_vma=False
    )
```

profile of v0, /device:TPU:0, one launch (start us, length us, event | category | flops | bytes accessed | tf_op | source)
XLA Modules:
  0.0 202.3 jit_solution(16404926073839543372)
XLA Ops:
  7.2 0.9 copy.22
  9.1 1.1 reduce-window.6
  10.7 0.9 constant_dynamic-slice_fusion
  11.8 4.9 %scatter_custom_fusion = bf16[768,512]{1,0:T(8,128)(2,1)S(1)} fusion(s32[512]{0:T(512)S(1)} %bitcast.76, bf16[128,512]{1,0:T(8,128)(2,1)S(1)} %constant_dynamic-slice_fusion, s32[1024]{0:T(1024)S(1)} %pad_clamp_fusion.1, bf16[]{:T(256)} %constant.69.clone.1), kind=kCustom, calls=%fused_computation.21 | custom fusion | bytes 786434 | tf_op jit(solution)/shard_map/scatter | solution.py:84
  16.7 27.2 %all_to_all.10 = bf16[8,96,512]{2,1,0:T(8,128)(2,1)} all-to-all(bf16[8,96,512]{2,1,0:T(8,128)(2,1)S(1)} %bitcast.71), channel_id=1, replica_groups=mesh['ep'=8,'tp'=4] {'ep'}, dimensions={0} | all-to-all | bytes 1572864 | tf_op jit(solution)/shard_map/all_to_all | solution.py:86
  44.0 42.8 %all-gather.3.cloned.1.call-done = bf16[8,96,2048]{2,1,0:T(8,128)(2,1)} async-done(((bf16[8,96,512]{2,1,0:T(8,128)(2,1)}), bf16[8,96,2048]{2,1,0:T(8,128)(2,1)}) %all-gather.3.cloned.1.call-update) | async-done | bytes 3145744 | tf_op jit(solution)/shard_map/all_gather | solution.py:87
  86.7 3.8 %fusion.4 = f32[8,96,512]{2,1,0:T(8,128)S(1)} fusion(bf16[8,96,2048]{2,1,0:T(8,128)(2,1)} %all-gather.3.cloned.1.call-done, bf16[1,2048,512]{2,1,0:T(8,128)(2,1)S(1)} %copy-done), kind=kOutput, calls=%fused_computation.7 | convolution fusion | flops 1610612736 | bytes 6815744 | tf_op jit(solution)/shard_map/secd,edf->secf/dot_general | solution.py:89
  90.6 2.8 %fusion.6 = bf16[8,1,96,512]{3,2,0,1:T(8,128)(2,1)} fusion(f32[8,96,512]{2,1,0:T(8,128)S(1)} %fusion.4, bf16[8,96,2048]{2,1,0:T(8,128)(2,1)S(1)} %copy-done.10, bf16[1,2048,512]{2,1,0:T(8,128)(2,1)S(1)} %copy-done.11), kind=kOutput, calls=%fused_computation.10 | convolution fusion | flops 1612972032 | bytes 7602176 | tf_op jit(solution)/shard_map/secd,edf->secf/dot_general | solution.py:92
  94.1 2.1 %collective-permute-start = (bf16[2,512]{1,0:T(2,128)(2,1)}, bf16[2,512]{1,0:T(2,128)(2,1)}, u32[]{:S(2)}, u32[]{:S(2)}) collective-permute-start(bf16[2,512]{1,0:T(2,128)(2,1)} %slice.40), channel_id=1, source_target_pairs={{0,4},{4,8},{8,12},{12,16},{16,20},{20,24},{24,28},{1,5},{5,9},{9,... | collective-permute-start | bytes 6152 | tf_op jit(solution)/shard_map/ppermute | solution.py:12
  96.9 2.8 %fusion.32 = f32[128,512]{1,0:T(8,128)} fusion(bf16[128,2048]{1,0:T(8,128)(2,1)S(1)} %copy-done.2, bf16[2048,512]{1,0:T(8,128)(2,1)} %param.31), kind=kOutput, calls=%fused_computation.73 | convolution fusion | flops 268435456 | bytes 2883584 | tf_op jit(solution)/shard_map/dot_general | solution.py:97
  99.6 37.7 %all-gather.5.cloned.1.call-done = bf16[768,2048]{1,0:T(8,128)(2,1)} async-done(((bf16[768,512]{1,0:T(8,128)(2,1)}), bf16[768,2048]{1,0:T(8,128)(2,1)}) %all-gather.5.cloned.1.call-update) | async-done | bytes 3145744 | tf_op jit(solution)/shard_map/all_gather | solution.py:100
  137.4 5.2 %fusion.12 = bf16[8,96,512]{2,1,0:T(8,128)(2,1)} fusion(bf16[8,96,2048]{2,1,0:T(8,128)(2,1)} %bitcast.80, bf16[1,2048,512]{2,1,0:T(8,128)(2,1)} %param.30), kind=kOutput, calls=%fused_computation.16 | convolution fusion | flops 1611005952 | bytes 6029312 | tf_op jit(solution)/shard_map/secf,efd->secd/dot_general | solution.py:103
  142.6 4.6 %all-to-all-start.1 = ((bf16[8,96,512]{2,1,0:T(8,128)(2,1)}), bf16[8,96,512]{2,1,0:T(8,128)(2,1)S(1)}, u32[]{:S(2)}, u32[]{:S(2)}) async-start(bf16[8,96,512]{2,1,0:T(8,128)(2,1)} %fusion.12), calls=%async_computation.1 | async-start | bytes 1572864 | tf_op jit(solution)/shard_map/all_to_all | solution.py:113
  148.4 2.1 %fusion.15 = bf16[128,512]{1,0:T(8,128)(2,1)S(1)} fusion(bf16[128,2048]{1,0:T(8,128)(2,1)S(1)} %copy-done.2, bf16[2048,512]{1,0:T(8,128)(2,1)} %param.32, f32[128,512]{1,0:T(8,128)} %fusion.32), kind=kOutput, calls=%fused_computation.19 | convolution fusion | flops 268828672 | bytes 3014656 | tf_op jit(solution)/shard_map/dot_general | solution.py:98
  150.4 11.2 %all_gather.15 = bf16[128,2048]{1,0:T(8,128)(2,1)} all-gather(bf16[128,512]{1,0:T(8,128)(2,1)S(1)} %fusion.15), channel_id=1, replica_groups=mesh['ep'=8,'tp'=4] {'tp'}, dimensions={1}, use_global_device_ids=true | all-gather | bytes 655360 | tf_op jit(solution)/shard_map/all_gather | solution.py:106
  162.4 1.4 convert_element_type.109
  165.9 1.1 fusion.22
  166.9 10.4 %all_gather.12 = bf16[128,2048]{1,0:T(8,128)(2,1)S(1)} all-gather(bf16[128,512]{1,0:T(8,128)(2,1)S(1)} %fusion.22), channel_id=1, replica_groups=mesh['ep'=8,'tp'=4] {'tp'}, dimensions={1}, use_global_device_ids=true | all-gather | bytes 655360 | tf_op jit(solution)/shard_map/all_gather | solution.py:65
  177.9 2.6 %gather_fusion = bf16[512,512]{1,0:T(8,128)(2,1)} fusion(bf16[768,512]{1,0:T(8,128)(2,1)S(1)} %bitcast.70, s32[1024]{0:T(1024)S(1)} %pad_clamp_fusion), kind=kCustom, calls=%fused_computation.1 | custom fusion | bytes 1050624 | tf_op jit(solution)/shard_map/gather | solution.py:114
  180.5 1.4 reshape.183
  182.6 2.3 %fusion.30 = (f32[128]{0:T(128)S(1)}, f32[128]{0:T(128)S(1)}, f32[128,512]{1,0:T(8,128)S(1)}) fusion(f32[128,512]{1,0:T(8,128)S(1)} %multiply_reduce_fusion, bf16[128,2048]{1,0:T(8,128)(2,1)} %all_gather.15, bf16[2048,512]{1,0:T(8,128)(2,1)} %param.33), kind=kOutput, calls=%fused_computation.71 | convolution fusion | flops 268697344 | bytes 3146752 | tf_op jit(solution)/shard_map/dot_general | solution.py:105
  184.9 8.9 %all-reduce = (f32[128]{0:T(128)S(1)}, f32[128]{0:T(128)S(1)}, f32[128]{0:T(128)S(1)}, f32[128]{0:T(128)S(1)}) all-reduce(f32[128]{0:T(128)S(1)} %get-tuple-element.5, f32[128]{0:T(128)S(1)} %get-tuple-element.4, f32[128]{0:T(128)S(1)} %get-tuple-element.3, f32[128]{0:T(128)S(1)} %get-tuple-element.2), channel_id=1, replica_groups=mesh['ep'=8,'tp'=4] {'tp'}, use_global_device_ids=true, to_apply=%region_3.4 | all-reduce | flops 512 | bytes 4096 | tf_op jit(solution)/shard_map/psum | solution.py:117
  193.9 0.8 add_convert_fusion
  194.7 0.8 add_convert_fusion.1
  (58 shorter events, 8.1 us)
Async XLA Ops:
  7.2 79.6 %copy-start = (bf16[1,2048,512]{2,1,0:T(8,128)(2,1)S(1)}, bf16[1,2048,512]{2,1,0:T(8,128)(2,1)}, u32[]{:S(2)}) copy-start(bf16[1,2048,512]{2,1,0:T(8,128)(2,1)} %param.28) | copy-start | bytes 6291460
  7.2 79.6 %all-gather.3.cloned.1.call-start = ((), (), s32[]{:S(2)}) async-start(), calls=%async_computation.2 | async-start | bytes 3932160 | tf_op jit(solution)/shard_map/all_gather | solution.py:87
  43.9 93.4 %all-gather.5.cloned.1.call-start = ((), (), s32[]{:S(2)}) async-start(), calls=%async_computation.3 | async-start | bytes 3932160 | tf_op jit(solution)/shard_map/all_gather | solution.py:100
  86.7 3.8 %copy-start.10 = (bf16[8,96,2048]{2,1,0:T(8,128)(2,1)S(1)}, bf16[8,96,2048]{2,1,0:T(8,128)(2,1)}, u32[]{:S(2)}) copy-start(bf16[8,96,2048]{2,1,0:T(8,128)(2,1)} %all-gather.3.cloned.1.call-done) | copy-start | bytes 9437188
  86.7 3.8 %copy-start.11 = (bf16[1,2048,512]{2,1,0:T(8,128)(2,1)S(1)}, bf16[1,2048,512]{2,1,0:T(8,128)(2,1)}, u32[]{:S(2)}) copy-start(bf16[1,2048,512]{2,1,0:T(8,128)(2,1)} %param.29) | copy-start | bytes 6291460
  90.6 2.9 %copy-start.4 = (bf16[128,512]{1,0:T(8,128)(2,1)S(1)}, bf16[128,512]{1,0:T(8,128)(2,1)}, u32[]{:S(2)}) copy-start(bf16[128,512]{1,0:T(8,128)(2,1)} %param.20) | copy-start | bytes 393220
  90.6 2.9 %copy-start.5 = (bf16[128,512]{1,0:T(8,128)(2,1)S(1)}, bf16[128,512]{1,0:T(8,128)(2,1)}, u32[]{:S(2)}) copy-start(bf16[128,512]{1,0:T(8,128)(2,1)} %param.19) | copy-start | bytes 393220
  90.6 6.3 %copy-start.2 = (bf16[128,2048]{1,0:T(8,128)(2,1)S(1)}, bf16[128,2048]{1,0:T(8,128)(2,1)}, u32[]{:S(2)}) copy-start(bf16[128,2048]{1,0:T(8,128)(2,1)} %param.25) | copy-start | bytes 1572868
  94.1 71.0 %collective-permute-start = (bf16[2,512]{1,0:T(2,128)(2,1)}, bf16[2,512]{1,0:T(2,128)(2,1)}, u32[]{:S(2)}, u32[]{:S(2)}) collective-permute-start(bf16[2,512]{1,0:T(2,128)(2,1)} %slice.40), channel_id=1, source_target_pairs={{0,4},{4,8},{8,12},{12,16},{16,20},{20,24},{24,28},{1,5},{5,9},{9,... | collective-permute-start | bytes 6152 | tf_op jit(solution)/shard_map/ppermute | solution.py:12
  137.4 10.4 %copy-start.6 = (bf16[3,512]{1,0:T(4,128)(2,1)S(1)}, bf16[3,512]{1,0:T(4,128)(2,1)}, u32[]{:S(2)}) copy-start(bf16[3,512]{1,0:T(4,128)(2,1)} %param.21) | copy-start | bytes 9220
  142.6 35.3 %all-to-all-start.1 = ((bf16[8,96,512]{2,1,0:T(8,128)(2,1)}), bf16[8,96,512]{2,1,0:T(8,128)(2,1)S(1)}, u32[]{:S(2)}, u32[]{:S(2)}) async-start(bf16[8,96,512]{2,1,0:T(8,128)(2,1)} %fusion.12), calls=%async_computation.1 | async-start | bytes 1572864 | tf_op jit(solution)/shard_map/all_to_all | solution.py:113
  147.2 14.4 %copy-start.8 = (f32[128,4]{0,1:T(4,128)S(1)}, f32[128,4]{0,1:T(4,128)}, u32[]{:S(2)}) copy-start(f32[128,4]{0,1:T(4,128)} %param.27) | copy-start | bytes 6148
  148.4 14.0 %copy-start.9 = (bf16[512]{0:T(512)(128)(2,1)S(1)}, bf16[512]{0:T(512)(128)(2,1)}, u32[]{:S(2)}) copy-start(bf16[512]{0:T(512)(128)(2,1)} %param.34) | copy-start | bytes 3076
  162.4 14.9 %copy-start.1 = (bf16[2048,512]{1,0:T(8,128)(2,1)S(1)}, bf16[2048,512]{1,0:T(8,128)(2,1)}, u32[]{:S(2)}) copy-start(bf16[2048,512]{1,0:T(8,128)(2,1)} %param.22) | copy-start | bytes 6291460
  177.9 4.0 %copy-start.3 = (f32[128,4]{1,0:T(8,128)S(1)}, f32[128,4]{1,0:T(8,128)}, u32[]{:S(2)}) copy-start(f32[128,4]{1,0:T(8,128)} %copy.24) | copy-start | bytes 6148
  181.9 12.0 %copy-start.7 = (f32[512]{0:T(512)S(1)}, f32[512]{0:T(512)}, u32[]{:S(2)}) copy-start(f32[512]{0:T(512)} %convert_element_type.109) | copy-start | bytes 6148
Sparse Core Ops, SparseCore 0:
  44.1 42.6 all-gather.2
  93.6 43.7 all-gather.4
where the time goes:
time: 203 us; the launch traced here: 202 us
  waiting for transfers between devices  80.5 us (40%)
  blocking collectives  57.7 us (28%)
  matrix products  19.5 us (10%)
  between operations  14.3 us (7%)
  local copies, waits for them, and re-layouts  12.8 us (6%)
  other arithmetic  10.6 us (5%)
  starting transfers between devices  6.82 us (3%)
    all_gather x1, waiting for transfers between devices, on_device(): arrived = lax.all_gather(arrived, 'tp', axis=2, tiled=True)  42.8 us
    all_gather x1, waiting for transfers between devices, on_device(): piece = lax.all_gather(flat_hidden, 'tp', axis=1, tiled=True)  37.7 us
    all_to_all x1, blocking collectives, on_device(): lax.all_to_all(sectioned, 'ep', split_axis=0, concat_axis=0, tiled=True)  27.2 us
    all_gather x1, blocking collectives, on_device(): lax.all_gather(shared_hidden, 'tp', axis=1, tiled=True)  11.2 us
    all_gather x1, blocking collectives, on_device(): lax.all_gather(weighted_in, 'tp', axis=1, tiled=True)  10.4 us
    psum x1, blocking collectives, on_device(): lax.psum((jnp.sum(mixed, axis=1), jnp.sum(mixed * mixed, axis=1), jnp.sum...  8.95 us
    dot_general x1, matrix products, on_device(): jnp.einsum('secf,efd->secd', shaped, block, preferred_element_type=jnp.fl...  5.22 us
    scatter x1, local copies, waits for them, and re-layouts, on_device(): buffer_rows = buffer_rows.at[targets].set(sent_rows[sources])  4.94 us
  transfers between devices with their start and end apart: 4, of which 2 were waited for; matrix products, arithmetic and copies ran while one was open for 9% of the time, Pallas kernels for 0%

commit v1 on v0

--- a/solution.py
+++ b/solution.py
@@ -97,7 +97,12 @@
     shared_gate_value = jnp.dot(moe_input, shared_gate, preferred_element_type=jnp.float32)
     shared_up_value = jnp.dot(moe_input, shared_up, preferred_element_type=jnp.float32)
     shared_hidden = (jax.nn.silu(shared_gate_value) * shared_up_value).astype(jnp.bfloat16)
-    piece = lax.all_gather(flat_hidden, "tp", axis=1, tiled=True)
+    ring = [flat_hidden]
+    for hop in range(3):
+        ring.append(lax.ppermute(ring[-1], "tp", [(dev, (dev + 1) % 4) for dev in range(4)]))
+    piece = jnp.roll(
+        jnp.concatenate(ring[::-1], axis=1), (lax.axis_index("tp") + 1) * ring[0].shape[1], axis=1
+    )
     block = expert_down
     shaped = piece.reshape(ep_count, local_experts, capacity, piece.shape[1])
     routed_sum = jnp.einsum("secf,efd->secd", shaped, block, preferred_element_type=jnp.float32)

time: 203 us -> 222 us (1.094)
  waiting for transfers between devices: 80.5 us -> 92.8 us
  local copies, waits for them, and re-layouts: 12.8 us -> 20.7 us
  matrix products: 19.5 us -> 16.1 us
    ppermute x0 -> x3, waiting for transfers between devices: none -> 50 us  [on_device(): lax.ppermute(ring[-1], 'tp', [(dev, (dev + 1) % 4) for dev in range(4)])]
    all_gather x1 -> x0, waiting for transfers between devices: 37.7 us -> none  [on_device(): piece = lax.all_gather(flat_hidden, 'tp', axis=1, tiled=True)]
    unnamed x26 -> x39, local copies, waits for them, and re-layouts: 1.73 us -> 9.29 us
    dot_general x1, matrix products: 5.22 us -> 2.66 us  [on_device(): jnp.einsum('secf,efd->secd', shaped, block, preferred_element_type=jnp.fl...]
  transfers between devices with their start and end apart: 4 -> 6, of which waited for: 2 -> 4; matrix products, arithmetic and copies ran while one was open for 9% -> 10% of each run, Pallas kernels for 0% -> 0%
where the time goes in v1:
time: 222 us; the launch traced here: 221 us
  waiting for transfers between devices  92.8 us (42%)
  blocking collectives  57.6 us (26%)
  local copies, waits for them, and re-layouts  20.7 us (9%)
  matrix products  16.1 us (7%)
  between operations  14.3 us (6%)
  other arithmetic  10.6 us (5%)
  starting transfers between devices  8.65 us (4%)
    ppermute x3, waiting for transfers between devices, on_device(): lax.ppermute(ring[-1], 'tp', [(dev, (dev + 1) % 4) for dev in range(4)])  50 us
    all_gather x1, waiting for transfers between devices, on_device(): arrived = lax.all_gather(arrived, 'tp', axis=2, tiled=True)  42.8 us
    all_to_all x1, blocking collectives, on_device(): lax.all_to_all(sectioned, 'ep', split_axis=0, concat_axis=0, tiled=True)  27.2 us
    all_gather x1, blocking collectives, on_device(): lax.all_gather(shared_hidden, 'tp', axis=1, tiled=True)  11.1 us
    all_gather x1, blocking collectives, on_device(): lax.all_gather(weighted_in, 'tp', axis=1, tiled=True)  10.4 us
    unnamed x39, local copies, waits for them, and re-layouts  9.29 us
    psum x1, blocking collectives, on_device(): lax.psum((jnp.sum(mixed, axis=1), jnp.sum(mixed * mixed, axis=1), jnp.sum...  8.93 us
    scatter x1, local copies, waits for them, and re-layouts, on_device(): buffer_rows = buffer_rows.at[targets].set(sent_rows[sources])  4.94 us
  transfers between devices with their start and end apart: 6, of which 4 were waited for; matrix products, arithmetic and copies ran while one was open for 10% of the time, Pallas kernels for 0%

profile of v1, /device:TPU:0, one launch (start us, length us, event | category | flops | bytes accessed | tf_op | source)
XLA Modules:
  0.0 220.8 jit_solution(9216590964737494213)
XLA Ops:
  11.8 4.9 %scatter_custom_fusion = bf16[768,512]{1,0:T(8,128)(2,1)S(1)} fusion(s32[512]{0:T(512)S(1)} %bitcast.79, bf16[128,512]{1,0:T(8,128)(2,1)S(1)} %constant_dynamic-slice_fusion.1, s32[1024]{0:T(1024)S(1)} %pad_clamp_fusion.1, bf16[]{:T(256)} %constant.88.clone.1), kind=kCustom, calls=%fused_computation.21 | custom fusion | bytes 786434 | tf_op jit(solution)/shard_map/scatter | solution.py:84
  16.7 27.2 %all_to_all.10 = bf16[8,96,512]{2,1,0:T(8,128)(2,1)} all-to-all(bf16[8,96,512]{2,1,0:T(8,128)(2,1)S(1)} %bitcast.75), channel_id=1, replica_groups=mesh['ep'=8,'tp'=4] {'ep'}, dimensions={0} | all-to-all | bytes 1572864 | tf_op jit(solution)/shard_map/all_to_all | solution.py:86
  43.9 42.8 %all-gather.2.cloned.1.call-done = bf16[8,96,2048]{2,1,0:T(8,128)(2,1)} async-done(((bf16[8,96,512]{2,1,0:T(8,128)(2,1)}), bf16[8,96,2048]{2,1,0:T(8,128)(2,1)}) %all-gather.2.cloned.1.call-update) | async-done | bytes 3145744 | tf_op jit(solution)/shard_map/all_gather | solution.py:87
  86.7 3.8 %fusion.4 = f32[8,96,512]{2,1,0:T(8,128)S(1)} fusion(bf16[8,96,2048]{2,1,0:T(8,128)(2,1)} %all-gather.2.cloned.1.call-done, bf16[1,2048,512]{2,1,0:T(8,128)(2,1)S(1)} %copy-done), kind=kOutput, calls=%fused_computation.7 | convolution fusion | flops 1610612736 | bytes 6815744 | tf_op jit(solution)/shard_map/secd,edf->secf/dot_general | solution.py:89
  90.6 2.0 fusion.6
  92.6 1.5 collective-permute-start.1
  94.1 18.5 %collective-permute-done.1 = bf16[768,512]{1,0:T(8,128)(2,1)S(1)} collective-permute-done((bf16[768,512]{1,0:T(8,128)(2,1)S(1)}, bf16[768,512]{1,0:T(8,128)(2,1)S(1)}, u32[]{:S(2)}, u32[]{:S(2)}) %collective-permute-start.1) | collective-permute-done | bytes 786464 | tf_op jit(solution)/shard_map/ppermute | solution.py:102
  114.1 18.7 %collective-permute-done.2 = bf16[768,512]{1,0:T(8,128)(2,1)} collective-permute-done((bf16[768,512]{1,0:T(8,128)(2,1)S(1)}, bf16[768,512]{1,0:T(8,128)(2,1)}, u32[]{:S(2)}, u32[]{:S(2)}) %collective-permute-start.2) | collective-permute-done | bytes 786464 | tf_op jit(solution)/shard_map/ppermute | solution.py:102
  133.5 1.9 collective-permute-start
  135.9 2.7 %fusion.32 = f32[128,512]{1,0:T(8,128)} fusion(bf16[128,2048]{1,0:T(8,128)(2,1)S(1)} %copy-done.4, bf16[2048,512]{1,0:T(8,128)(2,1)} %param.31), kind=kOutput, calls=%fused_computation.82 | convolution fusion | flops 268435456 | bytes 2883584 | tf_op jit(solution)/shard_map/dot_general | solution.py:97
  138.7 12.8 %collective-permute-done.3 = bf16[768,512]{1,0:T(8,128)(2,1)} collective-permute-done((bf16[768,512]{1,0:T(8,128)(2,1)}, bf16[768,512]{1,0:T(8,128)(2,1)}, u32[]{:S(2)}, u32[]{:S(2)}) %collective-permute-start.3) | collective-permute-done | bytes 786464 | tf_op jit(solution)/shard_map/ppermute | solution.py:102
  152.7 1.2 constant_dynamic-update-slice_fusion.6
  154.2 1.2 constant_dynamic-update-slice_fusion.3
  157.2 1.4 copy-done.14
  158.5 2.7 %fusion.12 = bf16[8,96,512]{2,1,0:T(8,128)(2,1)} fusion(bf16[8,96,2048]{2,1,0:T(8,128)(2,1)S(1)} %bitcast.71, bf16[1,2048,512]{2,1,0:T(8,128)(2,1)S(1)} %copy-done.14), kind=kOutput, calls=%fused_computation.16 | convolution fusion | flops 1611005952 | bytes 6029312 | tf_op jit(solution)/shard_map/secf,efd->secd/dot_general | solution.py:108
  161.2 4.6 %all-to-all-start.1 = ((bf16[8,96,512]{2,1,0:T(8,128)(2,1)}), bf16[8,96,512]{2,1,0:T(8,128)(2,1)S(1)}, u32[]{:S(2)}, u32[]{:S(2)}) async-start(bf16[8,96,512]{2,1,0:T(8,128)(2,1)} %fusion.12), calls=%async_computation.1 | async-start | bytes 1572864 | tf_op jit(solution)/shard_map/all_to_all | solution.py:118
  167.0 2.1 fusion.15
  169.1 11.1 %all_gather.11 = bf16[128,2048]{1,0:T(8,128)(2,1)} all-gather(bf16[128,512]{1,0:T(8,128)(2,1)S(1)} %fusion.15), channel_id=1, replica_groups=mesh['ep'=8,'tp'=4] {'tp'}, dimensions={1}, use_global_device_ids=true | all-gather | bytes 655360 | tf_op jit(solution)/shard_map/all_gather | solution.py:111
  180.9 1.4 convert_element_type.109
  185.5 10.4 %all_gather.9 = bf16[128,2048]{1,0:T(8,128)(2,1)S(1)} all-gather(bf16[128,512]{1,0:T(8,128)(2,1)S(1)} %fusion.22), channel_id=1, replica_groups=mesh['ep'=8,'tp'=4] {'tp'}, dimensions={1}, use_global_device_ids=true | all-gather | bytes 655360 | tf_op jit(solution)/shard_map/all_gather | solution.py:65
  196.4 2.6 %gather_fusion = bf16[512,512]{1,0:T(8,128)(2,1)} fusion(bf16[768,512]{1,0:T(8,128)(2,1)S(1)} %bitcast.70, s32[1024]{0:T(1024)S(1)} %pad_clamp_fusion), kind=kCustom, calls=%fused_computation.1 | custom fusion | bytes 1050624 | tf_op jit(solution)/shard_map/gather | solution.py:119
  199.1 1.4 reshape.183
  201.2 2.3 %fusion.30 = (f32[128]{0:T(128)S(1)}, f32[128]{0:T(128)S(1)}, f32[128,512]{1,0:T(8,128)S(1)}) fusion(f32[128,512]{1,0:T(8,128)S(1)} %multiply_reduce_fusion, bf16[128,2048]{1,0:T(8,128)(2,1)} %all_gather.11, bf16[2048,512]{1,0:T(8,128)(2,1)} %param.33), kind=kOutput, calls=%fused_computation.80 | convolution fusion | flops 268697344 | bytes 3146752 | tf_op jit(solution)/shard_map/dot_general | solution.py:110
  203.5 8.9 %all-reduce = (f32[128]{0:T(128)S(1)}, f32[128]{0:T(128)S(1)}, f32[128]{0:T(128)S(1)}, f32[128]{0:T(128)S(1)}) all-reduce(f32[128]{0:T(128)S(1)} %get-tuple-element.5, f32[128]{0:T(128)S(1)} %get-tuple-element.4, f32[128]{0:T(128)S(1)} %get-tuple-element.3, f32[128]{0:T(128)S(1)} %get-tuple-element.2), channel_id=1, replica_groups=mesh['ep'=8,'tp'=4] {'tp'}, use_global_device_ids=true, to_apply=%region_3.4 | all-reduce | flops 512 | bytes 4096 | tf_op jit(solution)/shard_map/psum | solution.py:122
  (76 shorter events, 18.3 us)
Async XLA Ops:
  7.2 79.6 %copy-start = (bf16[1,2048,512]{2,1,0:T(8,128)(2,1)S(1)}, bf16[1,2048,512]{2,1,0:T(8,128)(2,1)}, u32[]{:S(2)}) copy-start(bf16[1,2048,512]{2,1,0:T(8,128)(2,1)} %param.28) | copy-start | bytes 6291460
  7.2 79.6 %all-gather.2.cloned.1.call-start = ((), (), s32[]{:S(2)}) async-start(), calls=%async_computation.2 | async-start | bytes 3932160 | tf_op jit(solution)/shard_map/all_gather | solution.py:87
  86.7 3.8 %copy-start.12 = (bf16[8,96,2048]{2,1,0:T(8,128)(2,1)S(1)}, bf16[8,96,2048]{2,1,0:T(8,128)(2,1)}, u32[]{:S(2)}) copy-start(bf16[8,96,2048]{2,1,0:T(8,128)(2,1)} %all-gather.2.cloned.1.call-done) | copy-start | bytes 9437188
  86.7 3.8 %copy-start.13 = (bf16[1,2048,512]{2,1,0:T(8,128)(2,1)S(1)}, bf16[1,2048,512]{2,1,0:T(8,128)(2,1)}, u32[]{:S(2)}) copy-start(bf16[1,2048,512]{2,1,0:T(8,128)(2,1)} %param.29) | copy-start | bytes 6291460
  90.6 42.2 %copy-start.6 = (bf16[128,512]{1,0:T(8,128)(2,1)S(1)}, bf16[128,512]{1,0:T(8,128)(2,1)}, u32[]{:S(2)}) copy-start(bf16[128,512]{1,0:T(8,128)(2,1)} %param.20) | copy-start | bytes 393220
  90.6 42.2 %copy-start.7 = (bf16[128,512]{1,0:T(8,128)(2,1)S(1)}, bf16[128,512]{1,0:T(8,128)(2,1)}, u32[]{:S(2)}) copy-start(bf16[128,512]{1,0:T(8,128)(2,1)} %param.19) | copy-start | bytes 393220
  90.6 45.3 %copy-start.4 = (bf16[128,2048]{1,0:T(8,128)(2,1)S(1)}, bf16[128,2048]{1,0:T(8,128)(2,1)}, u32[]{:S(2)}) copy-start(bf16[128,2048]{1,0:T(8,128)(2,1)} %param.25) | copy-start | bytes 1572868
  92.6 20.1 %collective-permute-start.1 = (bf16[768,512]{1,0:T(8,128)(2,1)S(1)}, bf16[768,512]{1,0:T(8,128)(2,1)S(1)}, u32[]{:S(2)}, u32[]{:S(2)}) collective-permute-start(bf16[768,512]{1,0:T(8,128)(2,1)S(1)} %bitcast.72), channel_id=1, source_target_pairs={{0,1},{1,2},{2,3},{3,0},{4,5},{5,6},{6,7},{7,4},{8,9},{9,10},{10,1... | collective-permute-start | bytes 2359304 | tf_op jit(solution)/shard_map/ppermute | solution.py:102
  112.7 0.9 copy-start.1
  113.6 19.3 %collective-permute-start.2 = (bf16[768,512]{1,0:T(8,128)(2,1)S(1)}, bf16[768,512]{1,0:T(8,128)(2,1)}, u32[]{:S(2)}, u32[]{:S(2)}) collective-permute-start(bf16[768,512]{1,0:T(8,128)(2,1)S(1)} %collective-permute-done.1), channel_id=1, source_target_pairs={{0,1},{1,2},{2,3},{3,0},{4,5},{5,6},{6,7},{7,4},{8,9},{9,10},{10,1... | collective-permute-start | bytes 2359304 | tf_op jit(solution)/shard_map/ppermute | solution.py:102
  132.8 18.6 %collective-permute-start.3 = (bf16[768,512]{1,0:T(8,128)(2,1)}, bf16[768,512]{1,0:T(8,128)(2,1)}, u32[]{:S(2)}, u32[]{:S(2)}) collective-permute-start(bf16[768,512]{1,0:T(8,128)(2,1)} %collective-permute-done.2), channel_id=1, source_target_pairs={{0,1},{1,2},{2,3},{3,0},{4,5},{5,6},{6,7},{7,4},{8,9},{9,10},{10,1... | collective-permute-start | bytes 2359304 | tf_op jit(solution)/shard_map/ppermute | solution.py:102
  133.5 50.3 %collective-permute-start = (bf16[2,512]{1,0:T(2,128)(2,1)}, bf16[2,512]{1,0:T(2,128)(2,1)}, u32[]{:S(2)}, u32[]{:S(2)}) collective-permute-start(bf16[2,512]{1,0:T(2,128)(2,1)} %slice.40), channel_id=1, source_target_pairs={{0,4},{4,8},{8,12},{12,16},{16,20},{20,24},{24,28},{1,5},{5,9},{9,... | collective-permute-start | bytes 6152 | tf_op jit(solution)/shard_map/ppermute | solution.py:12
  138.7 15.3 %copy-start.2 = (bf16[768,512]{1,0:T(8,128)(2,1)S(1)}, bf16[768,512]{1,0:T(8,128)(2,1)}, u32[]{:S(2)}) copy-start(bf16[768,512]{1,0:T(8,128)(2,1)} %copy-done.1) | copy-start | bytes 2359300
  156.9 1.6 copy-start.14
  158.5 7.9 %copy-start.8 = (bf16[3,512]{1,0:T(4,128)(2,1)S(1)}, bf16[3,512]{1,0:T(4,128)(2,1)}, u32[]{:S(2)}) copy-start(bf16[3,512]{1,0:T(4,128)(2,1)} %param.21) | copy-start | bytes 9220
  161.2 35.2 %all-to-all-start.1 = ((bf16[8,96,512]{2,1,0:T(8,128)(2,1)}), bf16[8,96,512]{2,1,0:T(8,128)(2,1)S(1)}, u32[]{:S(2)}, u32[]{:S(2)}) async-start(bf16[8,96,512]{2,1,0:T(8,128)(2,1)} %fusion.12), calls=%async_computation.1 | async-start | bytes 1572864 | tf_op jit(solution)/shard_map/all_to_all | solution.py:118
  165.8 14.4 %copy-start.10 = (f32[128,4]{0,1:T(4,128)S(1)}, f32[128,4]{0,1:T(4,128)}, u32[]{:S(2)}) copy-start(f32[128,4]{0,1:T(4,128)} %param.27) | copy-start | bytes 6148
  167.0 14.0 %copy-start.11 = (bf16[512]{0:T(512)(128)(2,1)S(1)}, bf16[512]{0:T(512)(128)(2,1)}, u32[]{:S(2)}) copy-start(bf16[512]{0:T(512)(128)(2,1)} %param.34) | copy-start | bytes 3076
  180.9 14.9 %copy-start.3 = (bf16[2048,512]{1,0:T(8,128)(2,1)S(1)}, bf16[2048,512]{1,0:T(8,128)(2,1)}, u32[]{:S(2)}) copy-start(bf16[2048,512]{1,0:T(8,128)(2,1)} %param.22) | copy-start | bytes 6291460
  196.4 4.0 %copy-start.5 = (f32[128,4]{1,0:T(8,128)S(1)}, f32[128,4]{1,0:T(8,128)}, u32[]{:S(2)}) copy-start(f32[128,4]{1,0:T(8,128)} %copy.24) | copy-start | bytes 6148
  200.4 12.0 %copy-start.9 = (f32[512]{0:T(512)S(1)}, f32[512]{0:T(512)}, u32[]{:S(2)}) copy-start(f32[512]{0:T(512)} %convert_element_type.109) | copy-start | bytes 6148
Sparse Core Ops, SparseCore 0:
  44.1 42.6 all-gather.1
